TPU v7x, 32 devices: a whole 2x2x4 slice. The times are simulated.
32 devices in a mesh: rep: 2 (over x), fs: 8 (over z, y), tp: 2 (over core).
Axes of the slice: x: 2, y: 2, z: 4, core: 2. Of those that a mesh axis runs over, the one named last changes fastest.
Arguments:
- tokens: bfloat16 [12288, 2048], P(('rep', 'fs')), may hold values from -6 to 6
- norm_gain: float32 [2048], replicated, may hold values from 0.1 to 1.9
- up_weight: bfloat16 [2048, 8192], P('fs', 'tp'), may hold values from -0.125 to 0.125
- down_weight: bfloat16 [8192, 2048], P('tp', 'fs'), may hold values from -0.0625 to 0.0625
Outputs:
- layer_out: bfloat16 [12288, 2048], P(('rep', 'fs'), 'tp')
All inputs are finite; a program needn't handle non-finite values.
Results may differ from a plain program's by a relative error of at most 0.013.
Values may be sent and summed in bfloat16 or wider, within the bound.
A program may use at most 128 MiB of HBM per device.

v0:
```python
import functools

import jax
import jax.numpy as jnp
from jax import lax
from jax.experimental import pallas as pl
from jax.experimental.pallas import tpu as pltpu
from jax.sharding import PartitionSpec as P

MESH = pl.DeviceIdType.MESH
F32 = jnp.float32
BF16 = jnp.bfloat16


def kernel(nz, normed, up, down, out, T, acc, hid, U, Dn, Pr, Ar, Br, fin, loc, tok_s, tok_r,
           wy_s, wy_r, z_s, z_r, d_s, d_r, a_s, a_r, b_s, b_r, f_s, f_r):
    x, f, c = lax.axis_index("rep"), lax.axis_index("fs"), lax.axis_index("tp")
    z, y = f // 2, f % 2
    half, blk = T.shape[3], T.shape[4]
    wide = U.shape[2]
    row = blk // 2
    own = x * 2 + y
    ax, ay = (x + 1 - c) % 2, (y + c) % 2
    bx, by = (x + c) % 2, (y + 1 - c) % 2
    q_a, q_b, q_ab = ax * 2 + ay, bx * 2 + by, (1 - x) * 2 + 1 - y
    to_a = {"rep": ax, "fs": z * 2 + ay}
    to_b = {"rep": bx, "fs": z * 2 + by}
    to_y = {"fs": z * 2 + 1 - y}
    to_x = {"rep": 1 - x}
    to_c = {"tp": 1 - c}
    above = {"fs": jnp.minimum(z + 1, nz - 1) * 2 + y}
    below = {"fs": jnp.maximum(z - 1, 0) * 2 + y}
    has_above, has_below = z < nz - 1, z > 0

    def remote(src, dst, s, r, dev):
        return pltpu.make_async_remote_copy(
            src_ref=src, dst_ref=dst, send_sem=s, recv_sem=r, device_id=dev, device_id_type=MESH)

    def order(s):
        m = jnp.minimum(z, nz - 1 - z)
        near = z - (s + 1) // 2 if s % 2 else z + s // 2
        far = jnp.where(z < nz - 1 - z, s, nz - 1 - s)
        return jnp.where(s <= 2 * m, near, far)

    barrier = pltpu.get_barrier_semaphore()
    for dev in (to_x, to_y, to_c):
        pl.semaphore_signal(barrier, inc=1, device_id=dev, device_id_type=MESH)

    @pl.when(has_above)
    def _():
        pl.semaphore_signal(barrier, inc=1, device_id=above, device_id_type=MESH)

    @pl.when(has_below)
    def _():
        pl.semaphore_signal(barrier, inc=1, device_id=below, device_id_type=MESH)

    locals_ = []
    for k in range(nz):
        for h in range(2):
            locals_.append(pltpu.make_async_copy(
                normed.at[pl.ds(h * half, half), pl.ds(k * blk, blk)],
                T.at[k, own, h], loc.at[k * 2 + h]))
    slot = (lambda zz, p: U.at[zz, pl.ds(pl.multiple_of(p * row, row), row)],
            lambda zz, p: Dn.at[zz, :, pl.ds(pl.multiple_of(p * row, row), row)])
    part = (lambda q: up.at[:, pl.ds(pl.multiple_of(q * wide, wide), wide)],
            lambda q: down.at[pl.ds(pl.multiple_of(q * wide, wide), wide)])
    for w in range(2):
        locals_.append(pltpu.make_async_copy(part[w](own), slot[w](z, y), loc.at[2 * nz + w]))
    for copy in locals_:
        copy.start()
    pl.semaphore_wait(barrier, 3 + jnp.where(has_above, 1, 0) + jnp.where(has_below, 1, 0))

    swap = [remote(part[w](x * 2 + 1 - y), slot[w](z, y), wy_s.at[w], wy_r.at[w], to_y)
            for w in range(2)]

    def hop(w, upward, zz, p):
        return remote(slot[w](zz, p), slot[w](zz, p), z_s.at[w, 0 if upward else 1, zz, p],
                      z_r.at[w, zz, p], above if upward else below)

    def send(w, zz, p, act="start"):
        @pl.when(jnp.logical_and(has_above, zz <= z))
        def _():
            hop(w, True, zz, p).start() if act == "start" else hop(w, True, zz, p).wait_send()

        @pl.when(jnp.logical_and(has_below, zz >= z))
        def _():
            hop(w, False, zz, p).start() if act == "start" else hop(w, False, zz, p).wait_send()

    inner = jnp.logical_and(has_above, has_below)

    def pieces(w):
        return (y, 1 - y) if w == 0 else (0, 1)

    def relay(w, s):
        if s < nz:
            zz = order(s)
            for p in pieces(w):
                @pl.when(inner)
                def _():
                    hop(w, True, zz, p).wait_recv()
                send(w, zz, p)

    def arrived(w, s, p):
        @pl.when(jnp.logical_not(inner))
        def _():
            hop(w, True, order(s), p).wait_recv()

    def piece(q):
        return T.at[:, q, c]

    tok = [remote(piece(own), piece(own), tok_s.at[0], tok_r.at[0], to_a),
           remote(piece(own), piece(own), tok_s.at[1], tok_r.at[1], to_b),
           remote(piece(q_a), piece(q_a), tok_s.at[2], tok_r.at[2], to_b)]
    tok += [remote(piece(q), piece(q), tok_s.at[3 + i], tok_r.at[3 + i], to_c)
            for i, q in enumerate((q_a, q_b, q_ab))]

    def up_block(q, s):
        zz = order(s)

        @pl.loop(0, 2)
        def _(h):
            term = jnp.dot(T[zz, q, h], U[zz], preferred_element_type=F32)
            if s > 0:
                term += acc[q, h]
            if s < nz - 1:
                acc[q, h] = term
            else:
                hid[q, h] = jnp.square(jnp.maximum(term, 0.0)).astype(BF16)

    swap[0].start()
    swap[1].start()
    locals_[2 * nz].wait()
    send(0, z, y)
    for copy in locals_[:2 * nz]:
        copy.wait()
    tok[0].start()
    tok[1].start()
    swap[0].wait_recv()
    send(0, z, 1 - y)
    relay(0, 1)
    relay(0, 2)
    tok[0].wait_recv()
    tok[2].start()
    tok[3].start()
    locals_[2 * nz + 1].wait()
    swap[1].wait_recv()
    for s in range(3, nz):
        relay(0, s)
    send(1, z, 0)
    send(1, z, 1)
    up_block(own, 0)
    for p in pieces(0):
        arrived(0, 1, p)
    up_block(own, 1)
    tok[1].wait_recv()
    tok[4].start()
    for q, i in ((q_a, 4), (q_b, 3)):
        tok[i].wait_recv()
        up_block(q, 0)
        up_block(q, 1)
    relay(1, 1)
    for s in range(2, nz):
        for p in pieces(0):
            arrived(0, s, p)
        if s < nz - 1:
            for q in (own, q_a, q_b):
                up_block(q, s)
    relay(1, 2)
    tok[2].wait_recv()
    tok[5].start()
    if nz > 2:
        for q in (own, q_a, q_b):
            up_block(q, nz - 1)
    tok[5].wait_recv()
    for s in range(nz):
        up_block(q_ab, s)
    for s in range(3, nz):
        relay(1, s)
    for copy in tok:
        copy.wait_send()

    def cols(p):
        return pl.ds(p * row, row)

    def d2d(s, p):
        zz = order(s)
        return remote(T.at[zz, :, 1 - c, :, cols(p)], Pr.at[zz, :, :, cols(p)],
                      d_s.at[zz, p], d_r.at[zz, p], to_c)

    def to_first(s, p, i):
        zz = order(s)
        return remote(T.at[zz, (q_a, q_ab)[i], c, :, cols(p)], Ar.at[zz, i, :, cols(p)],
                      a_s.at[zz, p, i], a_r.at[zz, p, i], to_a)

    def to_second(s, p):
        zz = order(s)
        return remote(T.at[zz, q_b, c, :, cols(p)], Br.at[zz, :, cols(p)],
                      b_s.at[zz, p], b_r.at[zz, p], to_b)

    def finish(s, p):
        zz = order(s)
        return remote(T.at[zz, own, c, :, cols(p)], fin.at[zz % (nz // 2), c, :, cols(p)],
                      f_s.at[zz, p], f_r.at[zz, p], to_c)

    def stage_a(s, p):
        zz = order(s)
        for h in (1 - c, c):
            @pl.loop(0, 4)
            def _(q):
                T[zz, q, h, :, cols(p)] = jnp.dot(
                    hid[q, h], Dn[zz, :, cols(p)], preferred_element_type=F32).astype(BF16)
            if h is not c:
                d2d(s, p).start()

    def stage_b(s, p):
        zz, k = order(s), cols(p)
        d2d(s, p).wait_recv()
        for i, q in ((1, q_ab), (0, q_a), (2, q_b), (3, own)):
            T[zz, q, c, :, k] = (
                T[zz, q, c, :, k].astype(F32) + Pr[zz, q, :, k].astype(F32)).astype(BF16)
            if i < 2:
                to_first(s, p, i).start()

    def stage_c(s, p):
        zz, k = order(s), cols(p)
        to_first(s, p, 1).wait_recv()
        T[zz, q_b, c, :, k] = (
            T[zz, q_b, c, :, k].astype(F32) + Ar[zz, 1, :, k].astype(F32)).astype(BF16)
        to_second(s, p).start()

    def stage_d(s, p):
        zz, k = order(s), cols(p)
        to_first(s, p, 0).wait_recv()
        to_second(s, p).wait_recv()
        T[zz, own, c, :, k] = (
            T[zz, own, c, :, k].astype(F32) + Ar[zz, 0, :, k].astype(F32)
            + Br[zz, :, k].astype(F32)).astype(BF16)

        @pl.when(zz // (nz // 2) == c)
        def _():
            fin[zz % (nz // 2), c, :, k] = T[zz, own, c, :, k]

        @pl.when(zz // (nz // 2) != c)
        def _():
            finish(s, p).start()

    steps = [(s, p) for s in range(nz) for p in range(2)]
    for n, (s, p) in enumerate(steps):
        if s:
            arrived(1, s, p)
        stage_a(s, p)
        if n:
            stage_c(*steps[n - 1])
        stage_b(s, p)
        if n > 1:
            stage_d(*steps[n - 2])
    stage_d(*steps[-2])
    stage_c(*steps[-1])
    stage_d(*steps[-1])

    for s, p in steps:
        zz = order(s)

        @pl.when(zz // (nz // 2) == c)
        def _():
            finish(s, p).wait_recv()

        @pl.when(zz // (nz // 2) != c)
        def _():
            finish(s, p).wait_send()
    outs = [pltpu.make_async_copy(
        fin.at[k, h], out.at[pl.ds(h * half, half), pl.ds(k * blk, blk)], loc.at[k * 2 + h])
        for k in range(nz // 2) for h in range(2)]
    for copy in outs:
        copy.start()
    for w in range(2):
        swap[w].wait_send()
        for s in range(nz):
            for p in pieces(w):
                send(w, order(s), p, "wait")
    for s, p in steps:
        d2d(s, p).wait_send()
        to_first(s, p, 0).wait_send()
        to_first(s, p, 1).wait_send()
        to_second(s, p).wait_send()
    for copy in outs:
        copy.wait()


def fused(nz, normed, up, down):
    rows, d = normed.shape
    wide = up.shape[1] // 4
    half, blk = rows // 2, d // nz
    sem = pltpu.SemaphoreType.DMA
    return pl.pallas_call(
        functools.partial(kernel, nz),
        out_shape=jax.ShapeDtypeStruct((rows, d // 2), BF16),
        in_specs=[pl.BlockSpec(memory_space=pl.ANY)] * 3,
        out_specs=pl.BlockSpec(memory_space=pl.ANY),
        scratch_shapes=[
            pltpu.VMEM((nz, 4, 2, half, blk), BF16),
            pltpu.VMEM((4, 2, half, wide), F32),
            pltpu.VMEM((4, 2, half, wide), BF16),
            pltpu.VMEM((nz, blk, wide), BF16),
            pltpu.VMEM((nz, wide, blk), BF16),
            pltpu.VMEM((nz, 4, half, blk), BF16),
            pltpu.VMEM((nz, 2, half, blk), BF16),
            pltpu.VMEM((nz, half, blk), BF16),
            pltpu.VMEM((nz // 2, 2, half, blk), BF16),
            sem((2 * nz + 2,)), sem((6,)), sem((6,)), sem((2,)), sem((2,)),
            sem((2, 2, nz, 2)), sem((2, nz, 2)), sem((nz, 2)), sem((nz, 2)),
            sem((nz, 2, 2)), sem((nz, 2, 2)), sem((nz, 2)), sem((nz, 2)), sem((nz, 2)),
            sem((nz, 2)),
        ],
        compiler_params=pltpu.CompilerParams(
            collective_id=0, has_side_effects=True, vmem_limit_bytes=60 * 2**20),
    )(normed, up, down)


def spread(normed, up_weight, down_weight):
    n_rep = lax.axis_size("rep")
    rep = lax.axis_index("rep")
    ff = up_weight.shape[1] // n_rep
    up = lax.all_gather(
        lax.dynamic_slice_in_dim(up_weight, rep * ff, ff, 1), "fs", axis=0, tiled=True)
    down = lax.all_gather(
        lax.dynamic_slice_in_dim(down_weight, rep * ff, ff, 0), "fs", axis=1, tiled=True)
    normed = lax.all_gather(normed, "rep", axis=0, tiled=True)
    pre = jnp.dot(normed, up, preferred_element_type=F32)
    hidden = jnp.square(jax.nn.relu(pre)).astype(BF16)
    terms = jnp.dot(hidden, down, preferred_element_type=F32).astype(BF16)
    summed = lax.psum_scatter(terms, "tp", scatter_dimension=1, tiled=True)
    return lax.psum_scatter(summed, "rep", scatter_dimension=0, tiled=True)


def local(tokens, norm_gain, up_weight, down_weight):
    xf = tokens.astype(F32)
    inv_rms = lax.rsqrt(jnp.mean(xf * xf, axis=-1, keepdims=True) + 1e-06)
    normed = (xf * inv_rms * norm_gain).astype(BF16)
    n_rep, n_fs, n_tp = (lax.axis_size(a) for a in ("rep", "fs", "tp"))
    if n_rep == 2 and n_tp == 2 and n_fs % 4 == 0:
        summed = fused(n_fs // 2, normed, up_weight, down_weight)
    else:
        summed = spread(normed, up_weight, down_weight)
    summed = summed.astype(F32)
    width = summed.shape[1]
    own_cols = lax.dynamic_slice_in_dim(xf, lax.axis_index("tp") * width, width, 1)
    return (own_cols + summed).astype(BF16)


def solution(mesh):
    placed = (P(("rep", "fs"), None), P(), P("fs", "tp"), P("tp", "fs"))
    return jax.shard_map(
        local, mesh=mesh, in_specs=placed, out_specs=P(("rep", "fs"), "tp"), check_vma=False
    )
```

profile of v0, /device:TPU:1, one launch (start us, length us, event | category | flops | bytes accessed | tf_op | source)
XLA Modules:
  0.0 169.8 jit_solution(8624677188120161613)
XLA Ops:
  0.0 0.0 copy-start
  0.0 0.0 copy-start.2
  0.0 2.7 %multiply_reduce_fusion = f32[768]{0:T(1024)S(1)} fusion(bf16[768,2048]{1,0:T(8,128)(2,1)} %param.4), kind=kLoop, calls=%fused_computation.1 | loop fusion | flops 4717824 | bytes 3148800 | tf_op jit(solution)/shard_map/reduce_sum | solution.py:338
  2.7 0.1 copy-done
  2.8 0.0 copy-done.2
  2.8 2.4 %multiply_convert_fusion.normed = bf16[768,2048]{1,0:T(8,128)(2,1)} fusion(f32[2048]{0:T(1024)S(1)} %copy-done.2, f32[768]{0:T(1024)S(1)} %add_rsqrt_fusion, bf16[768,2048]{1,0:T(8,128)(2,1)S(1)} %copy-done), kind=kLoop, calls=%fused_computation | loop fusion | flops 6291456 | bytes 6302720 | tf_op jit(solution)/shard_map/convert_element_type | solution.py:339
  5.3 161.3 %shard_map.46 = bf16[768,1024]{1,0:T(8,128)(2,1)} custom-call(bf16[768,2048]{1,0:T(8,128)(2,1)} %multiply_convert_fusion.normed, bf16[256,4096]{1,0:T(8,128)(2,1)} %up.1, bf16[4096,256]{1,0:T(8,128)(2,1)} %down.1), custom_call_target="tpu_custom_call" | custom-call | tf_op jit(solution)/shard_map/pallas_call | solution.py:295
  166.6 0.0 copy-start.1
  166.6 0.8 convert_element_type.12
  167.5 0.6 copy-done.1
  168.0 1.7 %add_convert_fusion = bf16[768,1024]{1,0:T(8,128)(2,1)} fusion(bf16[768,1024]{1,0:T(8,128)(2,1)S(1)} %copy-done.1, f32[768,2048]{1,0:T(8,128)S(1)} %convert_element_type.12, s32[]{:T(128)S(6)} %select_n.3), kind=kLoop, calls=%fused_computation.2 | loop fusion | flops 2359296 | bytes 6291460 | tf_op jit(solution)/shard_map/convert_element_type | solution.py:348
  (1 shorter events, 0.0 us)
Async XLA Ops:
  0.0 2.8 %copy-start = (bf16[768,2048]{1,0:T(8,128)(2,1)S(1)}, bf16[768,2048]{1,0:T(8,128)(2,1)}, u32[]{:S(2)}) copy-start(bf16[768,2048]{1,0:T(8,128)(2,1)} %param.4) | copy-start | bytes 9437188
  0.0 2.8 %copy-start.2 = (f32[2048]{0:T(1024)S(1)}, f32[2048]{0:T(1024)}, u32[]{:S(2)}) copy-start(f32[2048]{0:T(1024)} %param.5) | copy-start | bytes 24580
  166.6 1.4 copy-start.1
where the time goes:
time: 170 us
  Pallas kernels  161 us (95%)
  other arithmetic  7.71 us (5%)
    pallas_call x1, Pallas kernels, fused(): pl.pallas_call(functools.partial(kernel, nz), out_shape=jax.ShapeDtypeStr...  161 us

commit v1 on v0

v1 whole, which is shorter than its diff:
```python
import functools

import jax
import jax.numpy as jnp
from jax import lax
from jax.experimental import pallas as pl
from jax.experimental.pallas import tpu as pltpu
from jax.sharding import PartitionSpec as P

MESH = pl.DeviceIdType.MESH
F32 = jnp.float32
BF16 = jnp.bfloat16


CHUNKS = 4
FORWARD_A = (3,)


def kernel(nz, eps, tokens, gain, up, down, out, T, acc, hid, U, Dn, Pr, Ar, Br, tokv, gv, loc,
           tok_s, tok_r, wu_s, wu_r, wd_s, wd_r, zu_s, zu_r, zd_s, zd_r, d_s, d_r, a_s, a_r, b_s, b_r,
           f_s, f_r):
    x, f, c = lax.axis_index("rep"), lax.axis_index("fs"), lax.axis_index("tp")
    z, y = f // 2, f % 2
    half, blk = T.shape[3], T.shape[4]
    wide = U.shape[2]
    row = blk // 2
    sub = row // 2
    own = x * 2 + y
    ax, ay = (x + 1 - c) % 2, (y + c) % 2
    bx, by = (x + c) % 2, (y + 1 - c) % 2
    q_a, q_b, q_ab = ax * 2 + ay, bx * 2 + by, (1 - x) * 2 + 1 - y
    to_a = {"rep": ax, "fs": z * 2 + ay}
    to_b = {"rep": bx, "fs": z * 2 + by}
    to_y = {"fs": z * 2 + 1 - y}
    to_x = {"rep": 1 - x}
    to_c = {"tp": 1 - c}
    above = {"fs": jnp.minimum(z + 1, nz - 1) * 2 + y}
    below = {"fs": jnp.maximum(z - 1, 0) * 2 + y}
    has_above, has_below = z < nz - 1, z > 0
    inner = jnp.logical_and(has_above, has_below)
    edge = jnp.logical_not(inner)

    def remote(src, dst, s, r, dev):
        return pltpu.make_async_remote_copy(
            src_ref=src, dst_ref=dst, send_sem=s, recv_sem=r, device_id=dev, device_id_type=MESH)

    def order(s):
        m = jnp.minimum(z, nz - 1 - z)
        near = z - (s + 1) // 2 if s % 2 else z + s // 2
        far = jnp.where(z < nz - 1 - z, s, nz - 1 - s)
        return jnp.where(s <= 2 * m, near, far)

    barrier = pltpu.get_barrier_semaphore()
    for dev in (to_x, to_y, to_c):
        pl.semaphore_signal(barrier, inc=1, device_id=dev, device_id_type=MESH)

    @pl.when(has_above)
    def _():
        pl.semaphore_signal(barrier, inc=1, device_id=above, device_id_type=MESH)

    @pl.when(has_below)
    def _():
        pl.semaphore_signal(barrier, inc=1, device_id=below, device_id_type=MESH)

    def up_part(q, k, n):
        return up.at[pl.ds(k * sub, n * sub), pl.ds(pl.multiple_of(q * wide, wide), wide)]

    def down_part(q):
        return down.at[pl.ds(pl.multiple_of(q * wide, wide), wide)]

    part = row // 2
    parts = ((0, row), (row, part), (row + part, part))

    def up_slot(zz, p, n=1):
        return U.at[zz, pl.ds(pl.multiple_of(p * sub, sub), n * sub)]

    def down_half(zz, p):
        return Dn.at[zz, :, pl.ds(pl.multiple_of(p * row, row), row)]

    def down_slot(zz, j):
        return Dn.at[zz, :, pl.ds(*parts[j])]

    load_up = pltpu.make_async_copy(up_part(own, 0, 2), up_slot(z, 2 * y, 2), loc.at[0])
    load_down = pltpu.make_async_copy(down_part(own), down_half(z, y), loc.at[1])
    load_gain = pltpu.make_async_copy(gain, gv, loc.at[2])
    load_tok = [pltpu.make_async_copy(
        tokens.at[pl.ds(pl.multiple_of(h * half, half), half)], tokv.at[h], loc.at[3 + i])
        for i, h in enumerate((c, 1 - c))]
    load_up.start()
    load_gain.start()
    for copy in load_tok:
        copy.start()
    load_down.start()
    pl.semaphore_wait(barrier, 3 + jnp.where(has_above, 1, 0) + jnp.where(has_below, 1, 0))

    up_order = (2 * y, 2 * y + 1, 2 * (1 - y), 2 * (1 - y) + 1)
    swap_up = [remote(up_part(x * 2 + 1 - y, k, 1), up_slot(z, 2 * y + k), wu_s.at[k], wu_r.at[k], to_y)
               for k in range(2)]
    swap_down = remote(down_part(x * 2 + 1 - y), down_half(z, y), wd_s.at[0], wd_r.at[0], to_y)

    def hop(w, upward, zz, p):
        slot, s, r = ((up_slot, zu_s, zu_r), (down_slot, zd_s, zd_r))[w]
        return remote(slot(zz, p), slot(zz, p), s.at[0 if upward else 1, zz, p],
                      r.at[zz, p], above if upward else below)

    def send(w, zz, p, act="start"):
        @pl.when(jnp.logical_and(has_above, zz <= z))
        def _():
            hop(w, True, zz, p).start() if act == "start" else hop(w, True, zz, p).wait_send()

        @pl.when(jnp.logical_and(has_below, zz >= z))
        def _():
            hop(w, False, zz, p).start() if act == "start" else hop(w, False, zz, p).wait_send()

    def relay(w, s, p):
        zz = order(s)

        @pl.when(inner)
        def _():
            hop(w, True, zz, p).wait_recv()
        send(w, zz, p)

    def arrived(w, s, p):
        @pl.when(edge)
        def _():
            hop(w, True, order(s), p).wait_recv()

    few = half // CHUNKS

    def piece(q, r):
        return T.at[:, q, c, pl.ds(r * few, few)]

    def tok(kind, r):
        if kind < 2:
            src, dev = piece(own, r), (to_a, to_b)[kind]
        elif kind == 2:
            flip = jnp.logical_and(c == 0, r in FORWARD_A)
            src = piece(jnp.where(flip, q_b, q_a), r)
            dev = {"rep": jnp.where(flip, ax, bx), "fs": z * 2 + jnp.where(flip, ay, by)}
        else:
            src, dev = piece((q_a, q_b, q_ab)[kind - 3], r), to_c
        return remote(src, src, tok_s.at[kind, r], tok_r.at[kind, r], dev)

    def norm(h, first, last):
        step = 16

        @pl.loop(first // step, last // step)
        def _(i):
            r = pl.ds(pl.multiple_of(i * step, step), step)
            xf = tokv[h, r, :].astype(F32)
            inv = lax.rsqrt(jnp.mean(xf * xf, axis=-1, keepdims=True) + eps)
            normed = (xf * inv * gv[...]).astype(BF16)
            for k in range(nz):
                T[k, own, h, r, :] = normed[:, k * blk:(k + 1) * blk]

    def up_blocks(blocks, s):
        zz = order(s)

        @pl.loop(0, 2 * len(blocks))
        def _(i):
            q, h = blocks[0], i % 2
            for n in range(1, len(blocks)):
                q = jnp.where(i // 2 == n, blocks[n], q)
            term = jnp.dot(T[zz, q, h], U[zz], preferred_element_type=F32)
            if s > 0:
                term += acc[q, h]
            if s < nz - 1:
                acc[q, h] = term
            else:
                hid[q, h] = jnp.square(jnp.maximum(term, 0.0)).astype(BF16)

    load_up.wait()
    for p in up_order[:2]:
        send(0, z, p)
    for copy in swap_up:
        copy.start()
    load_gain.wait()
    load_tok[0].wait()
    for r in range(CHUNKS):
        norm(c, r * few, (r + 1) * few)
        tok(0, r).start()
        tok(1, r).start()
    load_tok[1].wait()
    norm(1 - c, 0, half)
    for k in range(2):
        swap_up[k].wait_recv()
        send(0, z, up_order[2 + k])
    for p in up_order:
        for s in range(1, min(3, nz)):
            relay(0, s, p)
    up_blocks((own,), 0)
    rest = [(s, p) for s in range(3, nz) for p in up_order]
    for r in range(CHUNKS):
        for kind in range(2):
            tok(kind, r).wait_recv()
            tok(3 + kind, r).start()
        tok(2, r).start()
        for s, p in rest[r::CHUNKS]:
            relay(0, s, p)
    load_down.wait()
    swap_down.start()

    def send_half(p):
        @pl.when(p == 0)
        def _():
            send(1, z, 0)

        @pl.when(p == 1)
        def _():
            send(1, z, 1)
            send(1, z, 2)

    send_half(y)

    def edge_up(s):
        for p in up_order:
            arrived(0, s, p)

    edge_up(1)
    up_blocks((own,), 1)
    for r in range(CHUNKS):
        tok(3, r).wait_recv()
        tok(4, r).wait_recv()
    up_blocks((q_a, q_b), 0)
    up_blocks((q_a, q_b), 1)
    for s in range(2, nz - 1):
        edge_up(s)
        up_blocks((own, q_a, q_b), s)

    @pl.when(inner)
    def _():
        up_blocks((own, q_a, q_b), nz - 1)
    for r in range(CHUNKS):
        tok(2, r).wait_recv()
        tok(5, r).start()
    for r in range(CHUNKS):
        tok(5, r).wait_recv()
    for s in range(nz - 1):
        up_blocks((q_ab,), s)
    edge_up(nz - 1)

    @pl.when(inner)
    def _():
        up_blocks((q_ab,), nz - 1)

    @pl.when(edge)
    def _():
        up_blocks((own, q_a, q_b, q_ab), nz - 1)
    swap_down.wait_recv()
    send_half(1 - y)
    for r in range(CHUNKS):
        for kind in range(6):
            tok(kind, r).wait_send()

    def cols(p):
        return pl.ds(*p)

    def d2d(s, p):
        zz = order(s)
        return remote(T.at[zz, :, 1 - c, :, cols(p)], Pr.at[zz, :, :, cols(p)],
                      d_s.at[zz, tag(p)], d_r.at[zz, tag(p)], to_c)

    def to_first(s, p, i):
        zz = order(s)
        return remote(T.at[zz, (q_a, q_ab)[i], c, :, cols(p)], Ar.at[zz, i, :, cols(p)],
                      a_s.at[zz, tag(p), i], a_r.at[zz, tag(p), i], to_a)

    def to_second(s, p):
        zz = order(s)
        return remote(T.at[zz, q_b, c, :, cols(p)], Br.at[zz, :, cols(p)],
                      b_s.at[zz, tag(p)], b_r.at[zz, tag(p)], to_b)

    def place(s, p):
        k = order(s) % (nz // 2)
        return (pl.ds(pl.multiple_of(c * half, half), half),
                pl.ds(pl.multiple_of(k * blk + p[0], part), p[1]))

    def finish(s, p):
        zz = order(s)
        return remote(T.at[zz, own, c, :, cols(p)], out.at[place(s, p)],
                      f_s.at[zz, tag(p)], f_r.at[zz, tag(p)], to_c)

    def tag(p):
        return 2 if p[0] > row else p[0] // row

    def mine(s):
        return order(s) // (nz // 2) == c

    def stage_a(s, p):
        zz = order(s)
        for h in (1 - c, c):
            @pl.loop(0, 4, unroll=4)
            def _(q):
                T[zz, q, h, :, cols(p)] = jnp.dot(
                    hid[q, h], Dn[zz, :, cols(p)], preferred_element_type=F32).astype(BF16)
            if h is not c:
                d2d(s, p).start()

    def stage_b(s, p):
        zz, k = order(s), cols(p)
        d2d(s, p).wait_recv()
        for i, q in ((1, q_ab), (0, q_a), (2, q_b), (3, own)):
            T[zz, q, c, :, k] = (
                T[zz, q, c, :, k].astype(F32) + Pr[zz, q, :, k].astype(F32)).astype(BF16)
            if i < 2:
                to_first(s, p, i).start()

    def stage_c(s, p):
        zz, k = order(s), cols(p)
        to_first(s, p, 1).wait_recv()
        T[zz, q_b, c, :, k] = (
            T[zz, q_b, c, :, k].astype(F32) + Ar[zz, 1, :, k].astype(F32)).astype(BF16)
        to_second(s, p).start()

    def stage_d(s, p):
        zz, k = order(s), cols(p)
        to_first(s, p, 0).wait_recv()
        to_second(s, p).wait_recv()
        total = (tokv[c, :, pl.ds(pl.multiple_of(zz * blk + p[0], part), p[1])].astype(F32)
                 + T[zz, own, c, :, k].astype(F32) + Ar[zz, 0, :, k].astype(F32)
                 + Br[zz, :, k].astype(F32)).astype(BF16)

        @pl.when(mine(s))
        def _():
            out[place(s, p)] = total

        @pl.when(jnp.logical_not(mine(s)))
        def _():
            T[zz, own, c, :, k] = total
            finish(s, p).start()

    steps = [(s, p) for s in range(nz) for p in ((0, row), (row, row))]
    steps[-1:] = [(nz - 1, p) for p in parts[1:]]
    needs = [[j for j in range(3) if p[0] <= parts[j][0] < sum(p)] for _, p in steps]
    flat = [(s, j) for (s, _), js in zip(steps, needs) for j in js]
    relayed = set()

    def relay_until(s, j):
        for item in flat:
            if 0 < item[0] and item not in relayed and (item[0] < s or item[0] == s and item[1] <= j):
                relayed.add(item)
                relay(1, *item)

    for n, (s, p) in enumerate(steps):
        first = tag(p) == 0
        if s == 1:
            for j in needs[n]:
                relay(1, 1, j)
                relay(1, 2, j)
            relayed.update((k, j) for k in (1, 2) for j in needs[n])
        elif s > 1:
            relay_until(*((s, needs[n][-1]) if first or s == nz - 1 else (s + 1, 0)))
        if s:
            for j in needs[n]:
                arrived(1, s, j)
        stage_a(s, p)
        if n:
            stage_c(*steps[n - 1])
        stage_b(s, p)
        if n > 1:
            stage_d(*steps[n - 2])
    stage_c(*steps[-1])
    stage_d(*steps[-2])
    stage_d(*steps[-1])

    for copy in swap_up:
        copy.wait_send()
    swap_down.wait_send()
    for s in range(nz):
        for p in up_order:
            send(0, order(s), p, "wait")
        for j in range(3):
            send(1, order(s), j, "wait")
    for s, p in steps:
        d2d(s, p).wait_send()
        to_first(s, p, 0).wait_send()
        to_first(s, p, 1).wait_send()
        to_second(s, p).wait_send()

        @pl.when(mine(s))
        def _():
            finish(s, p).wait_recv()

        @pl.when(jnp.logical_not(mine(s)))
        def _():
            finish(s, p).wait_send()


def fused(nz, tokens, gain, up, down):
    rows, d = tokens.shape
    wide = up.shape[1] // 4
    half, blk = rows // 2, d // nz
    sem = pltpu.SemaphoreType.DMA
    return pl.pallas_call(
        functools.partial(kernel, nz, 1e-06),
        out_shape=pltpu.VMEM((rows, d // 2), BF16),
        in_specs=[pl.BlockSpec(memory_space=pl.ANY)] * 4,
        out_specs=pl.BlockSpec(memory_space=pltpu.VMEM),
        scratch_shapes=[
            pltpu.VMEM((nz, 4, 2, half, blk), BF16),
            pltpu.VMEM((4, 2, half, wide), F32),
            pltpu.VMEM((4, 2, half, wide), BF16),
            pltpu.VMEM((nz, blk, wide), BF16),
            pltpu.VMEM((nz, wide, blk), BF16),
            pltpu.VMEM((nz, 4, half, blk), BF16),
            pltpu.VMEM((nz, 2, half, blk), BF16),
            pltpu.VMEM((nz, half, blk), BF16),
            pltpu.VMEM((2, half, d), BF16),
            pltpu.VMEM((1, d), F32),
            sem((5,)), sem((6, CHUNKS)), sem((6, CHUNKS)), sem((2,)), sem((2,)), sem((1,)), sem((1,)),
            sem((2, nz, 4)), sem((nz, 4)), sem((2, nz, 3)), sem((nz, 3)), sem((nz, 3)), sem((nz, 3)),
            sem((nz, 3, 2)), sem((nz, 3, 2)), sem((nz, 3)), sem((nz, 3)), sem((nz, 3)),
            sem((nz, 3)),
        ],
        compiler_params=pltpu.CompilerParams(
            collective_id=0, has_side_effects=True, vmem_limit_bytes=58 * 2**20),
    )(tokens, gain.reshape(1, d), up, down)


def spread(normed, up_weight, down_weight):
    n_rep = lax.axis_size("rep")
    rep = lax.axis_index("rep")
    ff = up_weight.shape[1] // n_rep
    up = lax.all_gather(
        lax.dynamic_slice_in_dim(up_weight, rep * ff, ff, 1), "fs", axis=0, tiled=True)
    down = lax.all_gather(
        lax.dynamic_slice_in_dim(down_weight, rep * ff, ff, 0), "fs", axis=1, tiled=True)
    normed = lax.all_gather(normed, "rep", axis=0, tiled=True)
    pre = jnp.dot(normed, up, preferred_element_type=F32)
    hidden = jnp.square(jax.nn.relu(pre)).astype(BF16)
    terms = jnp.dot(hidden, down, preferred_element_type=F32).astype(BF16)
    summed = lax.psum_scatter(terms, "tp", scatter_dimension=1, tiled=True)
    return lax.psum_scatter(summed, "rep", scatter_dimension=0, tiled=True)


def local(tokens, norm_gain, up_weight, down_weight):
    n_rep, n_fs, n_tp = (lax.axis_size(a) for a in ("rep", "fs", "tp"))
    if n_rep == 2 and n_tp == 2 and n_fs % 4 == 0:
        got = fused(n_fs // 2, tokens, norm_gain, up_weight, down_weight)
        return got
    xf = tokens.astype(F32)
    inv_rms = lax.rsqrt(jnp.mean(xf * xf, axis=-1, keepdims=True) + 1e-06)
    normed = (xf * inv_rms * norm_gain).astype(BF16)
    summed = spread(normed, up_weight, down_weight).astype(F32)
    width = summed.shape[1]
    own_cols = lax.dynamic_slice_in_dim(xf, lax.axis_index("tp") * width, width, 1)
    return (own_cols + summed).astype(BF16)


def solution(mesh):
    placed = (P(("rep", "fs"), None), P(), P("fs", "tp"), P("tp", "fs"))
    return jax.shard_map(
        local, mesh=mesh, in_specs=placed, out_specs=P(("rep", "fs"), "tp"), check_vma=False
    )
```

time: 170 us -> 155 us (0.912)
  other arithmetic: 7.71 us -> 0 us
  Pallas kernels: 161 us -> 154 us
    pallas_call x1, Pallas kernels: 161 us -> 154 us  [fused(): pl.pallas_call(functools.partial(kernel, nz, 1e-06), out_shape=pltpu.VMEM...]
    convert_element_type x3 -> x0, other arithmetic: 4.99 us -> none  [the longest x1 2.44 us: local(): normed = (xf * inv_rms * norm_gain).astype(BF16)]
    reduce_sum x1 -> x0, other arithmetic: 2.72 us -> none  [local(): inv_rms = lax.rsqrt(jnp.mean(xf * xf, axis=-1, keepdims=True) + 1e-06)]
where the time goes in v1:
time: 155 us
  Pallas kernels  154 us (99%)
    pallas_call x1, Pallas kernels, fused(): pl.pallas_call(functools.partial(kernel, nz, 1e-06), out_shape=pltpu.VMEM...  154 us

profile of v1, /device:TPU:1, one launch (start us, length us, event | category | flops | bytes accessed | tf_op | source)
XLA Modules:
  0.0 155.1 jit_solution(12821831560132556610)
XLA Ops:
  0.0 153.9 %shard_map.46 = bf16[768,1024]{1,0:T(8,128)(2,1)S(1)} custom-call(bf16[768,2048]{1,0:T(8,128)(2,1)} %tokens.1, f32[1,2048]{1,0:T(1,128)} %bitcast.1, bf16[256,4096]{1,0:T(8,128)(2,1)} %up.1, bf16[4096,256]{1,0:T(8,128)(2,1)} %down.1), custom_call_target="tpu_custom_call" | custom-call | tf_op jit(solution)/shard_map/pallas_call | solution.py:394
  154.0 1.1 copy.6

commit v2 on v1

--- a/solution.py
+++ b/solution.py
@@ -14,11 +14,12 @@
 
 CHUNKS = 4
 FORWARD_A = (3,)
-
-
-def kernel(nz, eps, tokens, gain, up, down, out, T, acc, hid, U, Dn, Pr, Ar, Br, tokv, gv, loc,
-           tok_s, tok_r, wu_s, wu_r, wd_s, wd_r, zu_s, zu_r, zd_s, zd_r, d_s, d_r, a_s, a_r, b_s, b_r,
-           f_s, f_r):
+DEEP = 2
+
+
+def kernel(nz, eps, tokens, gain, up, down, out, T, acc, hid, U, Dn, Pr, Ar, Br, P2, A2, B2, tokv, gv, loc,
+           tok_s, tok_r, cor_r, w_s, w_r, z_s, zu_r, zd_r, d_r, a_r, b_r, out_s, f_r,
+           e_s, e_r):
     x, f, c = lax.axis_index("rep"), lax.axis_index("fs"), lax.axis_index("tp")
     z, y = f // 2, f % 2
     half, blk = T.shape[3], T.shape[4]
@@ -69,16 +70,21 @@
         return down.at[pl.ds(pl.multiple_of(q * wide, wide), wide)]
 
     part = row // 2
-    parts = ((0, row), (row, part), (row + part, part))
+    deep = wide * DEEP // 4
+    parts = ((0, row, 0, wide), (row, part, 0, wide), (row + part, part, 0, deep),
+             (row + part, part, deep, wide - deep))
 
     def up_slot(zz, p, n=1):
         return U.at[zz, pl.ds(pl.multiple_of(p * sub, sub), n * sub)]
 
+    def up_piece(zz, p):
+        return up_slot(zz, 2 * y, 2) if p == 0 else up_slot(zz, 2 * (1 - y) + p - 1)
+
     def down_half(zz, p):
         return Dn.at[zz, :, pl.ds(pl.multiple_of(p * row, row), row)]
 
     def down_slot(zz, j):
-        return Dn.at[zz, :, pl.ds(*parts[j])]
+        return Dn.at[zz, pl.ds(*parts[j][2:]), pl.ds(*parts[j][:2])]
 
     load_up = pltpu.make_async_copy(up_part(own, 0, 2), up_slot(z, 2 * y, 2), loc.at[0])
     load_down = pltpu.make_async_copy(down_part(own), down_half(z, y), loc.at[1])
@@ -93,24 +99,35 @@
     load_down.start()
     pl.semaphore_wait(barrier, 3 + jnp.where(has_above, 1, 0) + jnp.where(has_below, 1, 0))
 
-    up_order = (2 * y, 2 * y + 1, 2 * (1 - y), 2 * (1 - y) + 1)
-    swap_up = [remote(up_part(x * 2 + 1 - y, k, 1), up_slot(z, 2 * y + k), wu_s.at[k], wu_r.at[k], to_y)
+    up_order = (0, 1, 2)
+    swap_up = [remote(up_part(x * 2 + 1 - y, k, 1), up_slot(z, 2 * y + k), w_s.at[0], w_r.at[k], to_y)
                for k in range(2)]
-    swap_down = remote(down_part(x * 2 + 1 - y), down_half(z, y), wd_s.at[0], wd_r.at[0], to_y)
+    swap_down = remote(down_part(x * 2 + 1 - y), down_half(z, y), w_s.at[1], w_r.at[2], to_y)
 
     def hop(w, upward, zz, p):
-        slot, s, r = ((up_slot, zu_s, zu_r), (down_slot, zd_s, zd_r))[w]
-        return remote(slot(zz, p), slot(zz, p), s.at[0 if upward else 1, zz, p],
+        slot, r = ((up_piece, zu_r), (down_slot, zd_r))[w]
+        return remote(slot(zz, p), slot(zz, p), z_s.at[0 if upward else 1, zz],
                       r.at[zz, p], above if upward else below)
 
-    def send(w, zz, p, act="start"):
+    def send(w, zz, p):
         @pl.when(jnp.logical_and(has_above, zz <= z))
         def _():
-            hop(w, True, zz, p).start() if act == "start" else hop(w, True, zz, p).wait_send()
+            hop(w, True, zz, p).start()
 
         @pl.when(jnp.logical_and(has_below, zz >= z))
         def _():
-            hop(w, False, zz, p).start() if act == "start" else hop(w, False, zz, p).wait_send()
+            hop(w, False, zz, p).start()
+
+    def sent(zz):
+        both = U.at[pl.ds(0, 2)]
+
+        @pl.when(jnp.logical_and(has_above, zz <= z))
+        def _():
+            remote(both, both, z_s.at[0, zz], zu_r.at[0, 0], above).wait_send()
+
+        @pl.when(jnp.logical_and(has_below, zz >= z))
+        def _():
+            remote(both, both, z_s.at[1, zz], zu_r.at[0, 0], below).wait_send()
 
     def relay(w, s, p):
         zz = order(s)
@@ -139,7 +156,12 @@
             dev = {"rep": jnp.where(flip, ax, bx), "fs": z * 2 + jnp.where(flip, ay, by)}
         else:
             src, dev = piece((q_a, q_b, q_ab)[kind - 3], r), to_c
-        return remote(src, src, tok_s.at[kind, r], tok_r.at[kind, r], dev)
+        land = tok_r.at[kind, r] if kind < 3 else cor_r.at[kind - 3]
+        return remote(src, src, tok_s.at[0], land, dev)
+
+    def crossed(kind):
+        q = T.at[:, (q_b, q_a, q_ab)[kind - 3], 1 - c]
+        remote(q, q, tok_s.at[0], cor_r.at[kind - 3], to_c).wait_recv()
 
     def norm(h, first, last):
         step = 16
@@ -170,8 +192,7 @@
                 hid[q, h] = jnp.square(jnp.maximum(term, 0.0)).astype(BF16)
 
     load_up.wait()
-    for p in up_order[:2]:
-        send(0, z, p)
+    send(0, z, 0)
     for copy in swap_up:
         copy.start()
     load_gain.wait()
@@ -184,7 +205,7 @@
     norm(1 - c, 0, half)
     for k in range(2):
         swap_up[k].wait_recv()
-        send(0, z, up_order[2 + k])
+        send(0, z, 1 + k)
     for p in up_order:
         for s in range(1, min(3, nz)):
             relay(0, s, p)
@@ -207,8 +228,8 @@
 
         @pl.when(p == 1)
         def _():
-            send(1, z, 1)
-            send(1, z, 2)
+            for j in range(1, len(parts)):
+                send(1, z, j)
 
     send_half(y)
 
@@ -218,9 +239,8 @@
 
     edge_up(1)
     up_blocks((own,), 1)
-    for r in range(CHUNKS):
-        tok(3, r).wait_recv()
-        tok(4, r).wait_recv()
+    crossed(3)
+    crossed(4)
     up_blocks((q_a, q_b), 0)
     up_blocks((q_a, q_b), 1)
     for s in range(2, nz - 1):
@@ -233,8 +253,7 @@
     for r in range(CHUNKS):
         tok(2, r).wait_recv()
         tok(5, r).start()
-    for r in range(CHUNKS):
-        tok(5, r).wait_recv()
+    crossed(5)
     for s in range(nz - 1):
         up_blocks((q_ab,), s)
     edge_up(nz - 1)
@@ -248,27 +267,32 @@
         up_blocks((own, q_a, q_b, q_ab), nz - 1)
     swap_down.wait_recv()
     send_half(1 - y)
-    for r in range(CHUNKS):
-        for kind in range(6):
-            tok(kind, r).wait_send()
+    every = T.at[:, pl.ds(0, 3)]
+    remote(every, every, tok_s.at[0], cor_r.at[0], to_c).wait_send()
 
     def cols(p):
         return pl.ds(*p)
 
+    def step(s, p):
+        return 2 * s + tag(p)
+
+    def group(s, k):
+        return k if s < nz - 1 else 4 + k
+
     def d2d(s, p):
         zz = order(s)
         return remote(T.at[zz, :, 1 - c, :, cols(p)], Pr.at[zz, :, :, cols(p)],
-                      d_s.at[zz, tag(p)], d_r.at[zz, tag(p)], to_c)
+                      out_s.at[group(s, 0)], d_r.at[step(s, p)], to_c)
 
     def to_first(s, p, i):
         zz = order(s)
         return remote(T.at[zz, (q_a, q_ab)[i], c, :, cols(p)], Ar.at[zz, i, :, cols(p)],
-                      a_s.at[zz, tag(p), i], a_r.at[zz, tag(p), i], to_a)
+                      out_s.at[group(s, 1)], (b_r, a_r)[i].at[step(s, p)], to_a)
 
     def to_second(s, p):
         zz = order(s)
         return remote(T.at[zz, q_b, c, :, cols(p)], Br.at[zz, :, cols(p)],
-                      b_s.at[zz, tag(p)], b_r.at[zz, tag(p)], to_b)
+                      out_s.at[group(s, 2)], b_r.at[step(s, p)], to_b)
 
     def place(s, p):
         k = order(s) % (nz // 2)
@@ -278,7 +302,7 @@
     def finish(s, p):
         zz = order(s)
         return remote(T.at[zz, own, c, :, cols(p)], out.at[place(s, p)],
-                      f_s.at[zz, tag(p)], f_r.at[zz, tag(p)], to_c)
+                      out_s.at[3], f_r.at[0], to_c)
 
     def tag(p):
         return 2 if p[0] > row else p[0] // row
@@ -295,6 +319,94 @@
                     hid[q, h], Dn[zz, :, cols(p)], preferred_element_type=F32).astype(BF16)
             if h is not c:
                 d2d(s, p).start()
+
+    def stage_a_early(s, p):
+        zz = order(s)
+        for h in range(2):
+            @pl.loop(0, 4, unroll=4)
+            def _(q):
+                acc[q, h, :, :p[1]] = jnp.dot(
+                    hid[q, h, :, :deep], Dn[zz, :deep, cols(p)], preferred_element_type=F32)
+
+    def stage_a_late(s, p):
+        zz = order(s)
+        for h in range(2):
+            @pl.loop(0, 4, unroll=4)
+            def _(q):
+                T[zz, q, h, :, cols(p)] = (acc[q, h, :, :p[1]] + jnp.dot(
+                    hid[q, h, :, deep:], Dn[zz, deep:, cols(p)], preferred_element_type=F32)).astype(BF16)
+
+            @pl.when(c == 0)
+            def _():
+                gather_last(s, p, h).start()
+
+    def side(h):
+        px, py = (1 - x, y), (x, 1 - y)
+        (ax, ay), (bx, by) = (px, py) if h == 0 else (py, px)
+        return (ax * 2 + ay, bx * 2 + by, {"rep": ax, "fs": z * 2 + ay}, {"rep": bx, "fs": z * 2 + by})
+
+    def gather_last(s, p, h):
+        return remote(T.at[order(s), :, h, :, cols(p)], P2.at[h], e_s.at[h], e_r.at[h], to_c)
+
+    def first_last(s, p, h, i):
+        qa, _, dev, _ = side(h)
+        return remote(T.at[order(s), (qa, q_ab)[i], h, :, cols(p)], A2.at[h, i],
+                      e_s.at[2 + 2 * h + i], e_r.at[2 + 2 * h + i], dev)
+
+    def second_last(s, p, h):
+        _, qb, _, dev = side(h)
+        return remote(T.at[order(s), qb, h, :, cols(p)], B2.at[h], e_s.at[6 + h], e_r.at[6 + h], dev)
+
+    def out_last(s, p, h):
+        return (pl.ds(h * half, half),
+                pl.ds(pl.multiple_of(order(s) % (nz // 2) * blk + p[0], part), p[1]))
+
+    def finish_last(s, p, h):
+        return remote(T.at[order(s), own, h, :, cols(p)], out.at[out_last(s, p, h)],
+                      e_s.at[8 + h], e_r.at[8 + h], to_c)
+
+    def last_b(s, p):
+        zz, k = order(s), cols(p)
+        for h in range(2):
+            gather_last(s, p, h).wait_recv()
+            T[zz, q_ab, h, :, k] = (
+                T[zz, q_ab, h, :, k].astype(F32) + P2[h, q_ab].astype(F32)).astype(BF16)
+            first_last(s, p, h, 1).start()
+            for i, q in enumerate(side(h)[:2]):
+                T[zz, q, h, :, k] = (
+                    T[zz, q, h, :, k].astype(F32) + P2[h, q].astype(F32)).astype(BF16)
+                if i == 0:
+                    first_last(s, p, h, 0).start()
+
+    def last_c(s, p):
+        zz, k = order(s), cols(p)
+        for h in range(2):
+            qb = side(h)[1]
+            first_last(s, p, h, 1).wait_recv()
+            T[zz, qb, h, :, k] = (
+                T[zz, qb, h, :, k].astype(F32) + A2[h, 1].astype(F32)).astype(BF16)
+            second_last(s, p, h).start()
+
+    def last_d(s, p):
+        zz, k = order(s), cols(p)
+        for h in range(2):
+            T[zz, own, h, :, k] = (
+                T[zz, own, h, :, k].astype(F32) + P2[h, own].astype(F32)).astype(BF16)
+        for h in range(2):
+            first_last(s, p, h, 0).wait_recv()
+            second_last(s, p, h).wait_recv()
+            total = (tokv[h, :, pl.ds(pl.multiple_of(zz * blk + p[0], part), p[1])].astype(F32)
+                     + T[zz, own, h, :, k].astype(F32) + A2[h, 0].astype(F32)
+                     + B2[h].astype(F32)).astype(BF16)
+
+            @pl.when(mine(s))
+            def _():
+                out[out_last(s, p, h)] = total
+
+            @pl.when(jnp.logical_not(mine(s)))
+            def _():
+                T[zz, own, h, :, k] = total
+                finish_last(s, p, h).start()
 
     def stage_b(s, p):
         zz, k = order(s), cols(p)
@@ -314,8 +426,8 @@
 
     def stage_d(s, p):
         zz, k = order(s), cols(p)
-        to_first(s, p, 0).wait_recv()
-        to_second(s, p).wait_recv()
+        two = Ar.at[zz, :, :, k]
+        remote(two, two, out_s.at[1], b_r.at[step(s, p)], to_a).wait_recv()
         total = (tokv[c, :, pl.ds(pl.multiple_of(zz * blk + p[0], part), p[1])].astype(F32)
                  + T[zz, own, c, :, k].astype(F32) + Ar[zz, 0, :, k].astype(F32)
                  + Br[zz, :, k].astype(F32)).astype(BF16)
@@ -330,8 +442,8 @@
             finish(s, p).start()
 
     steps = [(s, p) for s in range(nz) for p in ((0, row), (row, row))]
-    steps[-1:] = [(nz - 1, p) for p in parts[1:]]
-    needs = [[j for j in range(3) if p[0] <= parts[j][0] < sum(p)] for _, p in steps]
+    steps[-1:] = [(nz - 1, p[:2]) for p in parts[1:3]]
+    needs = [[j for j in range(len(parts)) if p[0] <= parts[j][0] < sum(p)] for _, p in steps]
     flat = [(s, j) for (s, _), js in zip(steps, needs) for j in js]
     relayed = set()
 
@@ -340,6 +452,14 @@
             if 0 < item[0] and item not in relayed and (item[0] < s or item[0] == s and item[1] <= j):
                 relayed.add(item)
                 relay(1, *item)
+
+    last = len(steps) - 1
+
+    def ready(n, js):
+        s = steps[n][0]
+        if s:
+            for j in js:
+                arrived(1, s, j)
 
     for n, (s, p) in enumerate(steps):
         first = tag(p) == 0
@@ -348,42 +468,83 @@
                 relay(1, 1, j)
                 relay(1, 2, j)
             relayed.update((k, j) for k in (1, 2) for j in needs[n])
-        elif s > 1:
+        elif 1 < s and n < last:
             relay_until(*((s, needs[n][-1]) if first or s == nz - 1 else (s + 1, 0)))
-        if s:
-            for j in needs[n]:
-                arrived(1, s, j)
-        stage_a(s, p)
-        if n:
+        if n < last:
+            ready(n, needs[n])
+            stage_a(s, p)
+        else:
+            for j, stage in zip(needs[n], (stage_a_early, stage_a_late)):
+                relay_until(s, j)
+                ready(n, (j,))
+                stage(s, p)
+        if n and n < last:
             stage_c(*steps[n - 1])
-        stage_b(s, p)
-        if n > 1:
+        if n < last:
+            stage_b(s, p)
+        if 1 < n < last:
             stage_d(*steps[n - 2])
-    stage_c(*steps[-1])
-    stage_d(*steps[-2])
-    stage_d(*steps[-1])
-
-    for copy in swap_up:
-        copy.wait_send()
+
+    @pl.when(c == 1)
+    def _():
+        last_b(*steps[last])
+    stage_c(*steps[last - 1])
+    stage_d(*steps[last - 2])
+
+    @pl.when(c == 1)
+    def _():
+        last_c(*steps[last])
+    stage_d(*steps[last - 1])
+
+    @pl.when(c == 1)
+    def _():
+        last_d(*steps[last])
+    for zz in range(nz):
+        sent(zz)
+    ups = up_slot(0, 0, 2)
+    remote(ups, ups, w_s.at[0], w_r.at[0], to_y).wait_send()
     swap_down.wait_send()
-    for s in range(nz):
-        for p in up_order:
-            send(0, order(s), p, "wait")
-        for j in range(3):
-            send(1, order(s), j, "wait")
-    for s, p in steps:
-        d2d(s, p).wait_send()
-        to_first(s, p, 0).wait_send()
-        to_first(s, p, 1).wait_send()
-        to_second(s, p).wait_send()
-
-        @pl.when(mine(s))
-        def _():
-            finish(s, p).wait_recv()
-
-        @pl.when(jnp.logical_not(mine(s)))
-        def _():
-            finish(s, p).wait_send()
+
+    def all_sent(ref, k):
+        remote(ref, ref, out_s.at[k], d_r.at[0], to_c).wait_send()
+
+    for k, ref in enumerate((Pr, Ar, Br)):
+        all_sent(ref.at[pl.ds(0, nz - 1)], k)
+        lead = (0,) + (slice(None),) * (len(ref.shape) - 2)
+        all_sent(ref.at[(*lead, pl.ds(0, blk - part))], 4 + k)
+    far = mine(nz - 1)
+    most = out.at[pl.ds(0, half), pl.ds(0, (nz // 2) * blk - part)]
+    full = out.at[pl.ds(0, half)]
+
+    @pl.when(far)
+    def _():
+        all_sent(full, 3)
+        remote(most, most, out_s.at[3], f_r.at[0], to_c).wait_recv()
+
+    @pl.when(jnp.logical_not(far))
+    def _():
+        all_sent(most, 3)
+        remote(full, full, out_s.at[3], f_r.at[0], to_c).wait_recv()
+
+    end = steps[last]
+    for h in range(2):
+        @pl.when(c == 0)
+        def _():
+            gather_last(*end, h).wait_send()
+
+        @pl.when(c == 1)
+        def _():
+            for i in range(2):
+                first_last(*end, h, i).wait_send()
+            second_last(*end, h).wait_send()
+
+        @pl.when(jnp.logical_and(c == 1, jnp.logical_not(far)))
+        def _():
+            finish_last(*end, h).wait_send()
+
+        @pl.when(jnp.logical_and(c == 0, far))
+        def _():
+            finish_last(*end, h).wait_recv()
 
 
 def fused(nz, tokens, gain, up, down):
@@ -405,12 +566,14 @@
             pltpu.VMEM((nz, 4, half, blk), BF16),
             pltpu.VMEM((nz, 2, half, blk), BF16),
             pltpu.VMEM((nz, half, blk), BF16),
+            pltpu.VMEM((2, 4, half, blk // 4), BF16),
+            pltpu.VMEM((2, 2, half, blk // 4), BF16),
+            pltpu.VMEM((2, half, blk // 4), BF16),
             pltpu.VMEM((2, half, d), BF16),
             pltpu.VMEM((1, d), F32),
-            sem((5,)), sem((6, CHUNKS)), sem((6, CHUNKS)), sem((2,)), sem((2,)), sem((1,)), sem((1,)),
-            sem((2, nz, 4)), sem((nz, 4)), sem((2, nz, 3)), sem((nz, 3)), sem((nz, 3)), sem((nz, 3)),
-            sem((nz, 3, 2)), sem((nz, 3, 2)), sem((nz, 3)), sem((nz, 3)), sem((nz, 3)),
-            sem((nz, 3)),
+            sem((5,)), sem((1,)), sem((3, CHUNKS)), sem((3,)), sem((2,)), sem((3,)), sem((2, nz)),
+            sem((nz, 3)), sem((nz, 4)), sem((2 * nz + 1,)), sem((2 * nz + 1,)), sem((2 * nz + 1,)),
+            sem((7,)), sem((1,)), sem((10,)), sem((10,)),
         ],
         compiler_params=pltpu.CompilerParams(
             collective_id=0, has_side_effects=True, vmem_limit_bytes=58 * 2**20),

time: 155 us -> 153 us (0.987)
  Pallas kernels: 154 us -> 151 us
    pallas_call x1, Pallas kernels: 154 us -> 151 us  [fused(): pl.pallas_call(functools.partial(kernel, nz, 1e-06), out_shape=pltpu.VMEM...]
where the time goes in v2:
time: 153 us; the launch traced here: 152 us
  Pallas kernels  151 us (99%)
    pallas_call x1, Pallas kernels, fused(): pl.pallas_call(functools.partial(kernel, nz, 1e-06), out_shape=pltpu.VMEM...  151 us

profile of v2, /device:TPU:1, one launch (start us, length us, event | category | flops | bytes accessed | tf_op | source)
XLA Modules:
  0.0 152.4 jit_solution(14600752872358797317)
XLA Ops:
  0.0 151.2 %shard_map.46 = bf16[768,1024]{1,0:T(8,128)(2,1)S(1)} custom-call(bf16[768,2048]{1,0:T(8,128)(2,1)} %tokens.1, f32[1,2048]{1,0:T(1,128)} %bitcast.1, bf16[256,4096]{1,0:T(8,128)(2,1)} %up.1, bf16[4096,256]{1,0:T(8,128)(2,1)} %down.1), custom_call_target="tpu_custom_call" | custom-call | tf_op jit(solution)/shard_map/pallas_call | solution.py:555
  151.2 1.1 copy.6

commit v3 on v2

--- a/solution.py
+++ b/solution.py
@@ -461,6 +461,16 @@
             for j in js:
                 arrived(1, s, j)
 
+    def plan(n):
+        early = last - 3
+        todo = [("c", n - 1)] if n and n - 1 != early else []
+        todo.insert(0 if n == last - 1 else len(todo), ("b", n))
+        if n > 1:
+            todo.append(("d", n - 2))
+        if n == early:
+            todo.append(("c", n))
+        return todo
+
     for n, (s, p) in enumerate(steps):
         first = tag(p) == 0
         if s == 1:
@@ -478,12 +488,10 @@
                 relay_until(s, j)
                 ready(n, (j,))
                 stage(s, p)
-        if n and n < last:
-            stage_c(*steps[n - 1])
-        if n < last:
-            stage_b(s, p)
-        if 1 < n < last:
-            stage_d(*steps[n - 2])
+        if n == last:
+            break
+        for kind, m in plan(n):
+            {"b": stage_b, "c": stage_c, "d": stage_d}[kind](*steps[m])
 
     @pl.when(c == 1)
     def _():

time: 153 us -> 152 us (level)
  no operation moved by 1% of the time
where the time goes in v3:
time: 152 us
  Pallas kernels  151 us (99%)
    pallas_call x1, Pallas kernels, fused(): pl.pallas_call(functools.partial(kernel, nz, 1e-06), out_shape=pltpu.VMEM...  151 us

profile of v3, /device:TPU:1, one launch (start us, length us, event | category | flops | bytes accessed | tf_op | source)
XLA Modules:
  0.0 151.7 jit_solution(12525146911645733422)
XLA Ops:
  0.0 150.6 %shard_map.46 = bf16[768,1024]{1,0:T(8,128)(2,1)S(1)} custom-call(bf16[768,2048]{1,0:T(8,128)(2,1)} %tokens.1, f32[1,2048]{1,0:T(1,128)} %bitcast.1, bf16[256,4096]{1,0:T(8,128)(2,1)} %up.1, bf16[4096,256]{1,0:T(8,128)(2,1)} %down.1), custom_call_target="tpu_custom_call" | custom-call | tf_op jit(solution)/shard_map/pallas_call | solution.py:563
  150.6 1.1 copy.6

commit v4 on v3

--- a/solution.py
+++ b/solution.py
@@ -14,6 +14,8 @@
 
 CHUNKS = 4
 FORWARD_A = (3,)
+EARLY_FROM = 5
+SWAP = True
 DEEP = 2
 
 
@@ -328,34 +330,35 @@
                 acc[q, h, :, :p[1]] = jnp.dot(
                     hid[q, h, :, :deep], Dn[zz, :deep, cols(p)], preferred_element_type=F32)
 
+    q_x, q_y = (1 - x) * 2 + y, x * 2 + 1 - y
+
     def stage_a_late(s, p):
         zz = order(s)
-        for h in range(2):
-            @pl.loop(0, 4, unroll=4)
-            def _(q):
+        for i, q in enumerate((q_ab, q_x, q_y, own)):
+            for h in range(2):
                 T[zz, q, h, :, cols(p)] = (acc[q, h, :, :p[1]] + jnp.dot(
                     hid[q, h, :, deep:], Dn[zz, deep:, cols(p)], preferred_element_type=F32)).astype(BF16)
 
             @pl.when(c == 0)
             def _():
-                gather_last(s, p, h).start()
+                gather_last(s, p, q, i).start()
 
     def side(h):
         px, py = (1 - x, y), (x, 1 - y)
         (ax, ay), (bx, by) = (px, py) if h == 0 else (py, px)
         return (ax * 2 + ay, bx * 2 + by, {"rep": ax, "fs": z * 2 + ay}, {"rep": bx, "fs": z * 2 + by})
 
-    def gather_last(s, p, h):
-        return remote(T.at[order(s), :, h, :, cols(p)], P2.at[h], e_s.at[h], e_r.at[h], to_c)
+    def gather_last(s, p, q, i):
+        return remote(T.at[order(s), q, :, :, cols(p)], P2.at[i], e_s.at[0], e_r.at[i], to_c)
 
     def first_last(s, p, h, i):
         qa, _, dev, _ = side(h)
         return remote(T.at[order(s), (qa, q_ab)[i], h, :, cols(p)], A2.at[h, i],
-                      e_s.at[2 + 2 * h + i], e_r.at[2 + 2 * h + i], dev)
+                      e_s.at[1], e_r.at[4 + h if i else 6 + h], dev)
 
     def second_last(s, p, h):
         _, qb, _, dev = side(h)
-        return remote(T.at[order(s), qb, h, :, cols(p)], B2.at[h], e_s.at[6 + h], e_r.at[6 + h], dev)
+        return remote(T.at[order(s), qb, h, :, cols(p)], B2.at[h], e_s.at[2], e_r.at[6 + h], dev)
 
     def out_last(s, p, h):
         return (pl.ds(h * half, half),
@@ -363,20 +366,24 @@
 
     def finish_last(s, p, h):
         return remote(T.at[order(s), own, h, :, cols(p)], out.at[out_last(s, p, h)],
-                      e_s.at[8 + h], e_r.at[8 + h], to_c)
+                      e_s.at[3], e_r.at[8], to_c)
+
+    def join_last(s, p, q, i):
+        zz, k = order(s), cols(p)
+        gather_last(s, p, q, i).wait_recv()
+        for h in range(2):
+            T[zz, q, h, :, k] = (
+                T[zz, q, h, :, k].astype(F32) + P2[i, h].astype(F32)).astype(BF16)
 
     def last_b(s, p):
-        zz, k = order(s), cols(p)
-        for h in range(2):
-            gather_last(s, p, h).wait_recv()
-            T[zz, q_ab, h, :, k] = (
-                T[zz, q_ab, h, :, k].astype(F32) + P2[h, q_ab].astype(F32)).astype(BF16)
-            first_last(s, p, h, 1).start()
-            for i, q in enumerate(side(h)[:2]):
-                T[zz, q, h, :, k] = (
-                    T[zz, q, h, :, k].astype(F32) + P2[h, q].astype(F32)).astype(BF16)
-                if i == 0:
-                    first_last(s, p, h, 0).start()
+        join_last(s, p, q_ab, 0)
+        first_last(s, p, 0, 1).start()
+        first_last(s, p, 1, 1).start()
+        join_last(s, p, q_x, 1)
+        first_last(s, p, 0, 0).start()
+        join_last(s, p, q_y, 2)
+        first_last(s, p, 1, 0).start()
+        join_last(s, p, own, 3)
 
     def last_c(s, p):
         zz, k = order(s), cols(p)
@@ -390,11 +397,8 @@
     def last_d(s, p):
         zz, k = order(s), cols(p)
         for h in range(2):
-            T[zz, own, h, :, k] = (
-                T[zz, own, h, :, k].astype(F32) + P2[h, own].astype(F32)).astype(BF16)
-        for h in range(2):
-            first_last(s, p, h, 0).wait_recv()
-            second_last(s, p, h).wait_recv()
+            pair = A2.at[h]
+            remote(pair, pair, e_s.at[1], e_r.at[6 + h], to_c).wait_recv()
             total = (tokv[h, :, pl.ds(pl.multiple_of(zz * blk + p[0], part), p[1])].astype(F32)
                      + T[zz, own, h, :, k].astype(F32) + A2[h, 0].astype(F32)
                      + B2[h].astype(F32)).astype(BF16)
@@ -462,12 +466,12 @@
                 arrived(1, s, j)
 
     def plan(n):
-        early = last - 3
-        todo = [("c", n - 1)] if n and n - 1 != early else []
-        todo.insert(0 if n == last - 1 else len(todo), ("b", n))
+        early = range(EARLY_FROM, last - 2)
+        todo = [("c", n - 1)] if n and n - 1 not in early else []
+        todo.insert(0 if n == last - 1 and SWAP else len(todo), ("b", n))
         if n > 1:
             todo.append(("d", n - 2))
-        if n == early:
+        if n in early:
             todo.append(("c", n))
         return todo
 
@@ -534,25 +538,24 @@
         all_sent(most, 3)
         remote(full, full, out_s.at[3], f_r.at[0], to_c).wait_recv()
 
-    end = steps[last]
-    for h in range(2):
-        @pl.when(c == 0)
-        def _():
-            gather_last(*end, h).wait_send()
-
-        @pl.when(c == 1)
-        def _():
-            for i in range(2):
-                first_last(*end, h, i).wait_send()
-            second_last(*end, h).wait_send()
-
-        @pl.when(jnp.logical_and(c == 1, jnp.logical_not(far)))
-        def _():
-            finish_last(*end, h).wait_send()
-
-        @pl.when(jnp.logical_and(c == 0, far))
-        def _():
-            finish_last(*end, h).wait_recv()
+    far_rows = P2.at[3]
+
+    @pl.when(c == 0)
+    def _():
+        remote(P2, P2, e_s.at[0], e_r.at[0], to_c).wait_send()
+
+    @pl.when(c == 1)
+    def _():
+        remote(A2, A2, e_s.at[1], e_r.at[0], to_c).wait_send()
+        remote(B2, B2, e_s.at[2], e_r.at[0], to_c).wait_send()
+
+    @pl.when(jnp.logical_and(c == 1, jnp.logical_not(far)))
+    def _():
+        remote(far_rows, far_rows, e_s.at[3], e_r.at[0], to_c).wait_send()
+
+    @pl.when(jnp.logical_and(c == 0, far))
+    def _():
+        remote(far_rows, far_rows, e_s.at[3], e_r.at[8], to_c).wait_recv()
 
 
 def fused(nz, tokens, gain, up, down):
@@ -574,14 +577,14 @@
             pltpu.VMEM((nz, 4, half, blk), BF16),
             pltpu.VMEM((nz, 2, half, blk), BF16),
             pltpu.VMEM((nz, half, blk), BF16),
-            pltpu.VMEM((2, 4, half, blk // 4), BF16),
+            pltpu.VMEM((4, 2, half, blk // 4), BF16),
             pltpu.VMEM((2, 2, half, blk // 4), BF16),
             pltpu.VMEM((2, half, blk // 4), BF16),
             pltpu.VMEM((2, half, d), BF16),
             pltpu.VMEM((1, d), F32),
             sem((5,)), sem((1,)), sem((3, CHUNKS)), sem((3,)), sem((2,)), sem((3,)), sem((2, nz)),
-            sem((nz, 3)), sem((nz, 4)), sem((2 * nz + 1,)), sem((2 * nz + 1,)), sem((2 * nz + 1,)),
-            sem((7,)), sem((1,)), sem((10,)), sem((10,)),
+            sem((nz, 3)), sem((nz, 4)), sem((2 * nz,)), sem((2 * nz,)), sem((2 * nz,)),
+            sem((7,)), sem((1,)), sem((4,)), sem((9,)),
         ],
         compiler_params=pltpu.CompilerParams(
             collective_id=0, has_side_effects=True, vmem_limit_bytes=58 * 2**20),

time: 152 us -> 152 us (level)
  no operation moved by 1% of the time
where the time goes in v4:
time: 152 us
  Pallas kernels  151 us (99%)
    pallas_call x1, Pallas kernels, fused(): pl.pallas_call(functools.partial(kernel, nz, 1e-06), out_shape=pltpu.VMEM...  151 us

profile of v4, /device:TPU:1, one launch (start us, length us, event | category | flops | bytes accessed | tf_op | source)
XLA Modules:
  0.0 151.8 jit_solution(17461996407531606521)
XLA Ops:
  0.0 150.6 %shard_map.46 = bf16[768,1024]{1,0:T(8,128)(2,1)S(1)} custom-call(bf16[768,2048]{1,0:T(8,128)(2,1)} %tokens.1, f32[1,2048]{1,0:T(1,128)} %bitcast.1, bf16[256,4096]{1,0:T(8,128)(2,1)} %up.1, bf16[4096,256]{1,0:T(8,128)(2,1)} %down.1), custom_call_target="tpu_custom_call" | custom-call | tf_op jit(solution)/shard_map/pallas_call | solution.py:566
  150.6 1.1 copy.6
